TPU v7x, 32 devices: a whole 2x2x4 slice. The times are simulated.
32 devices in a mesh: grp: 2 (over y), fs: 4 (over z), tp: 4 (over x, core).
Axes of the slice: x: 2, y: 2, z: 4, core: 2. Of those that a mesh axis runs over, the one named last changes fastest.
Arguments:
- hidden_activations: bfloat16 [2048, 6144], P('tp', ('grp', 'fs')), parts along dimension 1, may hold values from -6 to 6
- attention_rescaling_factors: float32 [2048], replicated, may hold values from 0.1 to 1.9
- feature_rescaling_factors: float32 [2048], replicated, may hold values from 0.1 to 1.9
- request_matrix: float32 [2048, 2048], P('fs', 'tp'), may hold values from -0.125 to 0.125
- request_matrix_multipliers: float32 [2048], P('tp'), may hold values from 0.1 to 1.9
- lookup_matrix: float32 [2048, 2048], P('fs', 'tp'), may hold values from -0.125 to 0.125
- lookup_matrix_multipliers: float32 [2048], P('tp'), may hold values from 0.1 to 1.9
- content_matrix: float32 [2048, 4096], P('fs', 'tp'), may hold values from -0.125 to 0.125
- content_matrix_multipliers: float32 [4096], P('tp'), may hold values from 0.1 to 1.9
- valve_matrix: float32 [2048, 4096], P('fs', 'tp'), may hold values from -0.125 to 0.125
- valve_matrix_multipliers: float32 [4096], P('tp'), may hold values from 0.1 to 1.9
- result_matrix: float32 [4096, 2048], P('tp', 'fs'), may hold values from -0.09375 to 0.09375
- result_matrix_multipliers: float32 [2048], P('fs'), may hold values from 0.1 to 1.9
- expanding_matrix: float32 [2048, 8192], P('fs', 'tp'), may hold values from -0.125 to 0.125
- expand_matrix_multipliers: float32 [8192], P('tp'), may hold values from 0.1 to 1.9
- shrinking_matrix: float32 [8192, 2048], P('tp', 'fs'), may hold values from -0.0625 to 0.0625
- shrink_matrix_multipliers: float32 [2048], P('fs'), may hold values from 0.1 to 1.9
- attention_fading_logarithm: float32 [8], P('tp'), may hold values from -1 to 0
- spike_fading_logarithm: float32 [8, 6144], P('tp', ('grp', 'fs')), parts along dimension 1, may hold values from -1 to 0, as said below
Outputs:
- out_stream: bfloat16 [2048, 6144], P('tp', ('grp', 'fs')), parts along dimension 1
There are 2 independent parts, one for each index of `grp`. A program takes and returns all parts, laid end to end along the dimension named above; an argument that names none is the same for every part. Nothing has to cross between parts.
Inputs may be any that keep to these rules, and one draw needn't show every extreme that they name: `spike_fading_logarithm`: log decay added to the head's own.
All inputs are finite; a program needn't handle non-finite values.
Results may differ from a plain program's by a relative error of at most 0.019.
Values may be sent and summed in bfloat16 or wider, within the bound.
A program may use at most 128 MiB of HBM per device.

v0:
```python
import jax
import jax.numpy as jnp
from jax import lax
from jax.sharding import PartitionSpec as P

DK = 256
DV = 512
BLOCK_POSITIONS = 128


epsilon = 1e-06


def as_sent(value):

    def short(part):
        return part.astype(jnp.bfloat16) if part.dtype == jnp.float32 else part

    return jax.tree.map(short, value)


def rms_norm(matrix, norm_gain):
    values = matrix.astype(jnp.float32)
    factor = lax.rsqrt(jnp.mean(values * values, axis=0, keepdims=True) + epsilon)
    return (values * factor * norm_gain[:, None]).astype(jnp.bfloat16)


def project(normed, weight):
    return lax.dot_general(
        normed, weight, (((0,), (0,)), ((), ())), preferred_element_type=jnp.float32
    )


def collect_features(matrix):
    return lax.all_gather(matrix, "tp", axis=0, tiled=True)


def retain(query, keys, values, fading_logarithm_speed):
    length = query.shape[2]
    causal = jnp.arange(length)[:, None] >= jnp.arange(length)[None, :]

    def advance(memory, inputs):
        query_blk, key_blk, value_blk, rate_blk = inputs
        running = jnp.cumsum(rate_blk, axis=-1)
        closing = running[:, -1:]
        spread = jnp.where(causal, running[:, :, None] - running[:, None, :], 0.0)
        decays = jnp.where(causal, jnp.exp(spread), 0.0)
        scores = (
            jnp.einsum("gid,gjd->gij", query_blk, key_blk, preferred_element_type=jnp.float32)
            * decays
        )
        weights = scores.astype(jnp.bfloat16)
        within = jnp.einsum("gij,gjv->giv", weights, value_blk, preferred_element_type=jnp.float32)
        state_copy = memory.astype(jnp.bfloat16)
        carried = (
            jnp.einsum("gid,gdv->giv", query_blk, state_copy, preferred_element_type=jnp.float32)
            * jnp.exp(running)[:, :, None]
        )
        faded_keys = (key_blk.astype(jnp.float32) * jnp.exp(closing - running)[:, :, None]).astype(
            jnp.bfloat16
        )
        memory = memory * jnp.exp(closing)[:, :, None] + jnp.einsum(
            "gjd,gjv->gdv", faded_keys, value_blk, preferred_element_type=jnp.float32
        )
        return (memory, within + carried)

    initial = jnp.zeros((query.shape[0], query.shape[3], values.shape[3]), jnp.float32)
    stacked = tuple(
        (jnp.swapaxes(member, 0, 1) for member in (query, keys, values, fading_logarithm_speed))
    )
    _, outputs = lax.scan(advance, initial, stacked)
    return jnp.swapaxes(outputs, 0, 1)


def to_heads(matrix, width):
    token_inputs = matrix.shape[0]
    split = matrix.reshape(
        token_inputs // BLOCK_POSITIONS, BLOCK_POSITIONS, matrix.shape[1] // width, width
    )
    return jnp.transpose(split, (2, 0, 1, 3))


def group_norm(retained):
    center = jnp.mean(retained, axis=-1, keepdims=True)
    offset = retained - center
    variance = jnp.mean(offset * offset, axis=-1, keepdims=True)
    return offset * lax.rsqrt(variance + epsilon)


def squared_relu(summed, column_scale):
    rising = jax.nn.relu(summed * column_scale)
    return (rising * rising).astype(jnp.bfloat16)


def local(
    hidden_activations,
    attention_rescaling_factors,
    feature_rescaling_factors,
    request_matrix,
    request_matrix_multipliers,
    lookup_matrix,
    lookup_matrix_multipliers,
    content_matrix,
    content_matrix_multipliers,
    valve_matrix,
    valve_matrix_multipliers,
    result_matrix,
    result_matrix_multipliers,
    expanding_matrix,
    expand_matrix_multipliers,
    shrinking_matrix,
    shrink_matrix_multipliers,
    attention_fading_logarithm,
    spike_fading_logarithm,
):
    out_scales, down_scales = (
        lax.all_gather(result_matrix_multipliers, "fs", axis=0, tiled=True),
        lax.all_gather(shrink_matrix_multipliers, "fs", axis=0, tiled=True),
    )
    normed = rms_norm(collect_features(hidden_activations), attention_rescaling_factors)
    token_inputs = normed.shape[1]
    matrices = (request_matrix, lookup_matrix, content_matrix, valve_matrix)
    pieces = jax.tree.map(
        lambda part: lax.all_gather(part, "fs", axis=0, tiled=True),
        as_sent(tuple((matrix.astype(jnp.bfloat16) for matrix in matrices))),
    )
    picked = normed
    query_sum, key_sum, value_sum, gate_sum = tuple(
        (project(picked, segment) for segment in pieces)
    )
    query = (query_sum * request_matrix_multipliers).astype(jnp.bfloat16)
    keys = (key_sum * lookup_matrix_multipliers * DK ** (-0.5)).astype(jnp.bfloat16)
    values = (value_sum * content_matrix_multipliers).astype(jnp.bfloat16)
    gate = gate_sum * valve_matrix_multipliers
    shard_heads = attention_fading_logarithm.shape[0]
    fading_logarithm_speed = (attention_fading_logarithm[:, None] + spike_fading_logarithm).reshape(
        shard_heads, token_inputs // BLOCK_POSITIONS, BLOCK_POSITIONS
    )
    retained = retain(
        to_heads(query, DK), to_heads(keys, DK), to_heads(values, DV), fading_logarithm_speed
    )
    retained = jnp.transpose(retained, (1, 2, 0, 3)).reshape(token_inputs, shard_heads, DV)
    heads_out = (
        group_norm(retained).reshape(token_inputs, shard_heads * DV) * jax.nn.silu(gate)
    ).astype(jnp.bfloat16)
    out_whole = lax.all_gather(result_matrix.astype(jnp.bfloat16), "fs", axis=1, tiled=True)
    factors = out_scales
    update = lax.psum_scatter(
        (
            lax.dot_general(
                out_whole, heads_out, (((0,), (1,)), ((), ())), preferred_element_type=jnp.float32
            )
            * factors[:, None]
        ).astype(jnp.bfloat16),
        "tp",
        scatter_dimension=0,
        tiled=True,
    ).astype(jnp.float32)
    middle = (hidden_activations.astype(jnp.float32) + update).astype(jnp.bfloat16)
    normed_mlp = rms_norm(collect_features(middle), feature_rescaling_factors)
    picked = normed_mlp
    up_sum = project(
        picked, lax.all_gather(expanding_matrix.astype(jnp.bfloat16), "fs", axis=0, tiled=True)
    )
    hidden = squared_relu(up_sum, expand_matrix_multipliers)
    factors = down_scales
    terms = (
        lax.dot_general(
            lax.all_gather(shrinking_matrix.astype(jnp.bfloat16), "fs", axis=1, tiled=True),
            hidden,
            (((0,), (1,)), ((), ())),
            preferred_element_type=jnp.float32,
        )
        * factors[:, None]
    )
    lowered = lax.psum_scatter(
        terms.astype(jnp.bfloat16), "tp", scatter_dimension=0, tiled=True
    ).astype(jnp.float32)
    return (middle.astype(jnp.float32) + lowered).astype(jnp.bfloat16)


def solution(mesh):
    placed = (
        P("tp", ("grp", "fs")),
        P(),
        P(),
        P("fs", "tp"),
        P("tp"),
        P("fs", "tp"),
        P("tp"),
        P("fs", "tp"),
        P("tp"),
        P("fs", "tp"),
        P("tp"),
        P("tp", "fs"),
        P("fs"),
        P("fs", "tp"),
        P("tp"),
        P("tp", "fs"),
        P("fs"),
        P("tp"),
        P("tp", ("grp", "fs")),
    )
    return jax.shard_map(
        local, mesh=mesh, in_specs=placed, out_specs=P("tp", ("grp", "fs")), check_vma=False
    )
```

profile of v0, /device:TPU:0, one launch (start us, length us, event | category | flops | bytes accessed | tf_op | source)
XLA Modules:
  0.0 824.8 jit_solution(7764887072463206395)
XLA Ops:
  6.5 0.7 all-gather.12.cloned.1.call-update
  7.3 2.2 convert_element_type.93
  9.6 0.9 convert_element_type.97
  10.6 1.2 convert_element_type.95
  11.8 2.8 convert_element_type.99
  14.8 1.2 convert_element_type.101
  16.1 14.3 %all-gather = f32[4,1,512]{2,1,0:T(1,128)} all-gather(f32[1,1,512]{2,1,0:T(1,128)S(1)} %bitcast.91), channel_id=1, replica_groups=mesh['grp'=2,'fs'=4,'tp'=4] {'fs'}, dimensions={0}, use_global_device_ids=true | all-gather | bytes 10240 | tf_op jit(solution)/shard_map/all_gather | solution.py:117
  30.5 9.7 %all-gather.12.cloned.1.call-done = bf16[2048,768]{1,0:T(8,128)(2,1)} async-done(((bf16[512,768]{1,0:T(8,128)(2,1)}), bf16[2048,768]{1,0:T(8,128)(2,1)}) %all-gather.12.cloned.1.call-update) | async-done | bytes 3145744 | tf_op jit(solution)/shard_map/all_gather | solution.py:35
  40.2 2.6 fusion.39
  42.8 44.7 %all-gather.14.cloned.1.call-done = bf16[2048,512]{1,0:T(8,128)(2,1)} async-done(((bf16[512,512]{1,0:T(8,128)(2,1)}), bf16[2048,512]{1,0:T(8,128)(2,1)}) %all-gather.14.cloned.1.call-update) | async-done | bytes 2097168 | tf_op jit(solution)/shard_map/all_gather | solution.py:124
  87.4 4.5 multiply_convert_fusion.8
  92.1 41.4 %all-gather.18.cloned.1.call-done = bf16[2048,512]{1,0:T(8,128)(2,1)} async-done(((bf16[512,512]{1,0:T(8,128)(2,1)}), bf16[2048,512]{1,0:T(8,128)(2,1)}) %all-gather.18.cloned.1.call-update) | async-done | bytes 2097168 | tf_op jit(solution)/shard_map/all_gather | solution.py:124
  133.5 4.5 multiply_convert_fusion.7
  138.2 1.4 copy_bitcast_fusion.1
  139.6 74.9 %all-gather.16.cloned.1.call-done = bf16[2048,1024]{1,0:T(8,128)(2,1)} async-done(((bf16[512,1024]{1,0:T(8,128)(2,1)}), bf16[2048,1024]{1,0:T(8,128)(2,1)}) %all-gather.16.cloned.1.call-update) | async-done | bytes 4194320 | tf_op jit(solution)/shard_map/all_gather | solution.py:124
  214.5 6.9 multiply_convert_fusion.6
  221.4 2.6 reshape.102
  224.0 1.8 copy.51
  225.8 31.8 %while.14 = (s32[]{:T(128)}, f32[2,256,512]{2,1,0:T(8,128)S(1)}, f32[6,2,128,512]{3,2,1,0:T(8,128)}, f32[6,2,128]{2,1,0:T(2,128)S(1)}, bf16[6,2,128,256]{3,2,1,0...) while((s32[]{:T(128)}, f32[2,256,512]{2,1,0:T(8,128)S(1)}, ...), condition=%wide.region_3.4_spmd.clone.clone, body=%wide.region_1.3_spmd.clone.clone.sunk | while | flops 186269696 | bytes 5815448 | solution.py:71
  225.8 0.3 reduce_window_sum.14
  226.4 1.2 convolution_multiply_fusion.3
  227.5 2.1 fusion.83
  229.7 1.4 convolution_add_fusion.3
  231.7 1.2 convolution_multiply_fusion.3
  232.9 2.1 fusion.83
  235.0 1.4 convolution_add_fusion.3
  237.0 1.2 convolution_multiply_fusion.3
  238.2 2.1 fusion.83
  240.3 1.4 convolution_add_fusion.3
  242.3 1.2 convolution_multiply_fusion.3
  243.5 2.1 fusion.83
  245.6 1.4 convolution_add_fusion.3
  247.6 1.2 convolution_multiply_fusion.3
  248.8 2.1 fusion.83
  250.9 1.4 convolution_add_fusion.3
  252.9 1.2 convolution_multiply_fusion.3
  254.1 2.1 fusion.83
  256.2 1.4 convolution_add_fusion.3
  257.6 2.4 bitcast_reduce_fusion
  260.0 0.5 copy-done
  260.5 0.6 multiply_reduce_fusion
  261.2 1.1 mul.170
  262.3 2.4 copy.47
  264.9 1.1 sub.41
  265.9 2.4 copy.46
  268.4 2.4 copy.40
  270.9 2.4 copy.45
  273.3 21.9 %all-gather.20.cloned.1.call-done = bf16[2048,1024]{1,0:T(8,128)(2,1)} async-done(((bf16[512,1024]{1,0:T(8,128)(2,1)}), bf16[2048,1024]{1,0:T(8,128)(2,1)}) %all-gather.20.cloned.1.call-update) | async-done | bytes 4194320 | tf_op jit(solution)/shard_map/all_gather | solution.py:124
  295.2 80.7 %all-gather.22.cloned.1.call-done = bf16[1024,2048]{1,0:T(8,128)(2,1)} async-done(((bf16[1024,512]{1,0:T(8,128)(2,1)}), bf16[1024,2048]{1,0:T(8,128)(2,1)}) %all-gather.22.cloned.1.call-update) | async-done | bytes 4194320 | tf_op jit(solution)/shard_map/all_gather | solution.py:146
  375.9 15.5 %fusion.49 = bf16[2048,768]{0,1:T(8,128)(2,1)} fusion(f32[2048]{0:T(1024)S(1)} %bitcast.89, bf16[1024,2048]{1,0:T(8,128)(2,1)} %all-gather.22.cloned.1.call-done, f32[768,1024]{1,0:T(8,128)} %bitcast.86, f32[768,1024]{1,0:T(8,128)} %bitcast.88, f32[768,1024]{1,0:T(8,128)} %bitcast.87, bf16[2048,1024]{1,0:T(8,128)(2,1)} %all-gather.20.cloned.1.call-done, ...), kind=kOutput, calls=%fused_computation.63 | convolution fusion | flops 6458966016 | bytes 24140800 | tf_op jit(solution)/shard_map/dot_general | solution.py:150
  391.4 1.1 copy-done.4
  392.8 35.0 %reduce-scatter.3.cloned.1.call-done = bf16[512,768]{0,1:T(8,128)(2,1)} async-done(((bf16[2048,768]{0,1:T(8,128)(2,1)}), bf16[512,768]{0,1:T(8,128)(2,1)}) %reduce-scatter.3.cloned.1.call-update) | async-done | bytes 786448 | tf_op jit(solution)/shard_map/reduce_scatter | solution.py:148
  427.7 2.2 add_convert_fusion.1
  430.0 3.9 convert_element_type.109
  434.0 3.9 convert_element_type.111
  437.9 12.2 %all-gather.1 = f32[4,1,512]{2,1,0:T(1,128)S(1)} all-gather(f32[1,1,512]{2,1,0:T(1,128)S(1)} %bitcast.92), channel_id=1, replica_groups=mesh['grp'=2,'fs'=4,'tp'=4] {'fs'}, dimensions={0}, use_global_device_ids=true | all-gather | bytes 10240 | tf_op jit(solution)/shard_map/all_gather | solution.py:118
  450.1 8.6 %all-gather.24.cloned.1.call-done = bf16[2048,768]{0,1:T(8,128)(2,1)} async-done(((bf16[512,768]{0,1:T(8,128)(2,1)}), bf16[2048,768]{0,1:T(8,128)(2,1)}) %all-gather.24.cloned.1.call-update) | async-done | bytes 3145744 | tf_op jit(solution)/shard_map/all_gather | solution.py:35
  458.6 2.7 fusion.42
  461.4 148.5 %all-gather.26.cloned.1.call-done = bf16[2048,2048]{1,0:T(8,128)(2,1)} async-done(((bf16[512,2048]{1,0:T(8,128)(2,1)}), bf16[2048,2048]{1,0:T(8,128)(2,1)}) %all-gather.26.cloned.1.call-update) | async-done | bytes 8388624 | tf_op jit(solution)/shard_map/all_gather | solution.py:163
  609.9 149.2 %all-gather.28.cloned.1.call-done = bf16[2048,2048]{1,0:T(8,128)(2,1)} async-done(((bf16[2048,512]{1,0:T(8,128)(2,1)}), bf16[2048,2048]{1,0:T(8,128)(2,1)}) %all-gather.28.cloned.1.call-update) | async-done | bytes 8388624 | tf_op jit(solution)/shard_map/all_gather | solution.py:169
  759.1 20.6 %fusion.48 = bf16[2048,768]{0,1:T(8,128)(2,1)} fusion(f32[2048]{0:T(1024)S(1)} %bitcast.90, bf16[2048,2048]{1,0:T(8,128)(2,1)} %all-gather.28.cloned.1.call-done, bf16[2048,2048]{1,0:T(8,128)(2,1)} %all-gather.26.cloned.1.call-done, bf16[2048,768]{0,1:T(8,128)(2,1)S(1)} %copy-done.3, f32[2048]{0:T(1024)S(1)} %copy-done.17, f32[2048]{0:T(1024)S(1)} %copy-done.18, ...), kind=kOutput, calls=%fused_computation.62 | convolution fusion | flops 12900630528 | bytes 23096320 | tf_op jit(solution)/shard_map/dot_general | solution.py:168
  779.7 36.1 %reduce-scatter.5.cloned.1.call-done = bf16[512,768]{0,1:T(8,128)(2,1)} async-done(((bf16[2048,768]{0,1:T(8,128)(2,1)}), bf16[512,768]{0,1:T(8,128)(2,1)}) %reduce-scatter.5.cloned.1.call-update) | async-done | bytes 786448 | tf_op jit(solution)/shard_map/reduce_scatter | solution.py:176
  815.8 1.3 add_convert_fusion
  817.1 1.2 copy.43
  (106 shorter events, 5.0 us)
Async XLA Ops:
  6.5 3.1 copy-start.7
  6.5 4.0 copy-start.5
  6.5 33.6 %all-gather.12.cloned.1.call-start = ((), (), s32[]{:S(2)}) async-start(), calls=%async_computation.2 | async-start | bytes 3932160 | tf_op jit(solution)/shard_map/all_gather | solution.py:35
  7.3 80.2 %all-gather.14.cloned.1.call-start = ((), (), s32[]{:S(2)}) async-start(), calls=%async_computation.3 | async-start | bytes 2621440 | tf_op jit(solution)/shard_map/all_gather | solution.py:124
  9.6 123.9 %all-gather.18.cloned.1.call-start = ((), (), s32[]{:S(2)}) async-start(), calls=%async_computation.5 | async-start | bytes 2621440 | tf_op jit(solution)/shard_map/all_gather | solution.py:124
  10.5 204.0 %all-gather.16.cloned.1.call-start = ((), (), s32[]{:S(2)}) async-start(), calls=%async_computation.4 | async-start | bytes 5242880 | tf_op jit(solution)/shard_map/all_gather | solution.py:124
  11.8 3.0 copy-start.6
  11.8 283.4 %all-gather.20.cloned.1.call-start = ((), (), s32[]{:S(2)}) async-start(), calls=%async_computation.6 | async-start | bytes 5242880 | tf_op jit(solution)/shard_map/all_gather | solution.py:124
  14.7 1.4 copy-start.12
  14.7 15.7 %copy-start.9 = (f32[2,768]{1,0:T(2,128)S(1)}, f32[2,768]{1,0:T(2,128)}, u32[]{:S(2)}) copy-start(f32[2,768]{1,0:T(2,128)} %param.39) | copy-start | bytes 18436
  14.7 15.7 %copy-start.14 = (f32[2]{0:T(128)S(1)}, f32[2]{0:T(128)}, u32[]{:S(2)}) copy-start(f32[2]{0:T(128)} %param.38) | copy-start | bytes 28
  14.7 72.7 %copy-start.15 = (f32[2048]{0:T(1024)S(1)}, f32[2048]{0:T(1024)}, u32[]{:S(2)}) copy-start(f32[2048]{0:T(1024)} %param.22) | copy-start | bytes 24580
  14.7 72.7 %copy-start.21 = (f32[512]{0:T(512)S(1)}, f32[512]{0:T(512)}, u32[]{:S(2)}) copy-start(f32[512]{0:T(512)} %param.27) | copy-start | bytes 6148
  14.7 361.1 %all-gather.22.cloned.1.call-start = ((), (), s32[]{:S(2)}) async-start(), calls=%async_computation.7 | async-start | bytes 5242880 | tf_op jit(solution)/shard_map/all_gather | solution.py:146
  16.0 411.7 %reduce-scatter.3.cloned.1.call-start = ((), (), s32[]{:S(2)}) async-start(), calls=%async_computation.8 | async-start | bytes 3932160 | tf_op jit(solution)/shard_map/reduce_scatter | solution.py:148
  42.7 171.8 %copy-start.10 = (f32[768]{0:T(1024)}, f32[768]{0:T(1024)S(1)}, u32[]{:S(2)}) copy-start(f32[768]{0:T(1024)S(1)} %add_rsqrt_fusion.1) | copy-start | bytes 9220
  42.8 90.7 %copy-start.22 = (f32[512]{0:T(512)S(1)}, f32[512]{0:T(512)}, u32[]{:S(2)}) copy-start(f32[512]{0:T(512)} %param.25) | copy-start | bytes 6148
  138.0 76.5 %copy-start.19 = (f32[1024]{0:T(1024)S(1)}, f32[1024]{0:T(1024)}, u32[]{:S(2)}) copy-start(f32[1024]{0:T(1024)} %param.29) | copy-start | bytes 12292
  257.6 2.9 copy-start
  270.8 105.1 %copy-start.2 = (bf16[2048,768]{1,0:T(8,128)(2,1)S(1)}, bf16[2048,768]{1,0:T(8,128)(2,1)}, u32[]{:S(2)}) copy-start(bf16[2048,768]{1,0:T(8,128)(2,1)} %all-gather.12.cloned.1.call-done) | copy-start | bytes 9437188
  270.8 105.0 %copy-start.8 = (f32[4,1,512]{2,1,0:T(1,128)S(1)}, f32[4,1,512]{2,1,0:T(1,128)}, u32[]{:S(2)}) copy-start(f32[4,1,512]{2,1,0:T(1,128)} %all-gather) | copy-start | bytes 24580
  270.8 105.0 %copy-start.11 = (f32[768]{0:T(1024)S(1)}, f32[768]{0:T(1024)}, u32[]{:S(2)}) copy-start(f32[768]{0:T(1024)} %copy-done.10) | copy-start | bytes 9220
  270.8 105.0 %copy-start.16 = (f32[2048]{0:T(1024)S(1)}, f32[2048]{0:T(1024)}, u32[]{:S(2)}) copy-start(f32[2048]{0:T(1024)} %param.22) | copy-start | bytes 24580
  270.9 105.0 %copy-start.20 = (f32[1024]{0:T(1024)S(1)}, f32[1024]{0:T(1024)}, u32[]{:S(2)}) copy-start(f32[1024]{0:T(1024)} %param.31) | copy-start | bytes 12292
  391.3 1.1 copy-start.4
  391.4 67.3 %all-gather.24.cloned.1.call-start = ((), (), s32[]{:S(2)}) async-start(), calls=%async_computation.9 | async-start | bytes 3932160 | tf_op jit(solution)/shard_map/all_gather | solution.py:35
  430.0 179.9 %all-gather.26.cloned.1.call-start = ((), (), s32[]{:S(2)}) async-start(), calls=%async_computation.10 | async-start | bytes 10485760 | tf_op jit(solution)/shard_map/all_gather | solution.py:163
  433.9 4.0 copy-start.13
  433.9 325.2 %all-gather.28.cloned.1.call-start = ((), (), s32[]{:S(2)}) async-start(), calls=%async_computation.11 | async-start | bytes 10485760 | tf_op jit(solution)/shard_map/all_gather | solution.py:169
  437.8 321.3 %copy-start.17 = (f32[2048]{0:T(1024)S(1)}, f32[2048]{0:T(1024)}, u32[]{:S(2)}) copy-start(f32[2048]{0:T(1024)} %param.35) | copy-start | bytes 24580
  437.8 321.3 %copy-start.18 = (f32[2048]{0:T(1024)S(1)}, f32[2048]{0:T(1024)}, u32[]{:S(2)}) copy-start(f32[2048]{0:T(1024)} %param.23) | copy-start | bytes 24580
  437.9 377.9 %reduce-scatter.5.cloned.1.call-start = ((), (), s32[]{:S(2)}) async-start(), calls=%async_computation.12 | async-start | bytes 3932160 | tf_op jit(solution)/shard_map/reduce_scatter | solution.py:176
  458.6 300.5 %copy-start.3 = (bf16[2048,768]{0,1:T(8,128)(2,1)S(1)}, bf16[2048,768]{0,1:T(8,128)(2,1)}, u32[]{:S(2)}) copy-start(bf16[2048,768]{0,1:T(8,128)(2,1)} %all-gather.24.cloned.1.call-done) | copy-start | bytes 9437188
  779.7 36.1 %copy-start.1 = (bf16[512,768]{0,1:T(8,128)(2,1)S(1)}, bf16[512,768]{0,1:T(8,128)(2,1)}, u32[]{:S(2)}) copy-start(bf16[512,768]{0,1:T(8,128)(2,1)} %add_convert_fusion.1) | copy-start | bytes 2359300
Sparse Core Ops, SparseCore 0:
  8.9 31.2 all-gather.11
  41.7 45.6 all-gather.13
  89.0 44.4 all-gather.17
  134.9 79.5 all-gather.15
  215.9 79.2 all-gather.19
  296.6 79.2 all-gather.21
  391.5 36.1 reduce-scatter.2
  430.1 28.5 all-gather.23
  460.2 149.6 all-gather.25
  611.3 147.7 all-gather.27
  779.9 35.8 reduce-scatter.4
where the time goes:
time: 826 us; the launch traced here: 825 us
  waiting for transfers between devices  651 us (79%)
  matrix products  79.9 us (10%)
  other arithmetic  30.3 us (4%)
  blocking collectives  26.4 us (3%)
  local copies, waits for them, and re-layouts  22.6 us (3%)
  between operations  13.5 us (2%)
    all_gather x4, waiting for transfers between devices, local(): lax.all_gather(part, 'fs', axis=0, tiled=True)  183 us
    all_gather x1, waiting for transfers between devices, local(): lax.all_gather(shrinking_matrix.astype(jnp.bfloat16), 'fs', axis=1, tiled...  149 us
    all_gather x1, waiting for transfers between devices, local(): lax.all_gather(expanding_matrix.astype(jnp.bfloat16), 'fs', axis=0, tiled...  148 us
    all_gather x1, waiting for transfers between devices, local(): lax.all_gather(result_matrix.astype(jnp.bfloat16), 'fs', axis=1, tiled=True)  80.7 us
    reduce_scatter x1, waiting for transfers between devices, local(): lax.psum_scatter(terms.astype(jnp.bfloat16), 'tp', scatter_dimension=0, t...  36.1 us
    reduce_scatter x1, waiting for transfers between devices, local(): lax.psum_scatter((lax.dot_general(out_whole, heads_out, (((0,), (1,)), ((...  35 us
    dot_general x1, matrix products, local(): lax.dot_general(lax.all_gather(shrinking_matrix.astype(jnp.bfloat16), 'fs...  20.6 us
    all_gather x2, waiting for transfers between devices, collect_features(): return lax.all_gather(matrix, 'tp', axis=0, tiled=True)  18.2 us
  transfers between devices with their start and end apart: 11, of which 11 were waited for; matrix products, arithmetic and copies ran while one was open for 11% of the time, Pallas kernels for 0%

commit v1 on v0

v1 whole, which is shorter than its diff:
```python
import jax
import jax.numpy as jnp
from jax import lax
from jax.sharding import PartitionSpec as P


DK = 256
DV = 512


epsilon = 1e-06


def rms_norm(matrix, norm_gain):
    values = matrix.astype(jnp.float32)
    factor = lax.rsqrt(jnp.mean(values * values, axis=0, keepdims=True) + epsilon)
    return (values * factor * norm_gain[:, None]).astype(jnp.bfloat16)


def project(normed, weight):
    return lax.dot_general(
        normed, weight, (((0,), (0,)), ((), ())), preferred_element_type=jnp.float32
    )


def collect_features(matrix):
    return lax.all_gather(matrix, "tp", axis=0, tiled=True)


def group_norm(retained):
    center = jnp.mean(retained, axis=-1, keepdims=True)
    offset = retained - center
    variance = jnp.mean(offset * offset, axis=-1, keepdims=True)
    return offset * lax.rsqrt(variance + epsilon)


def retain(query, keys, values, rates):
    length, heads = query.shape[0], rates.shape[0]
    causal = jnp.arange(length)[:, None] >= jnp.arange(length)[None, :]
    running = jnp.cumsum(rates, axis=-1)
    outputs = []
    for head in range(heads):
        head_query = query[:, head * DK : (head + 1) * DK]
        head_keys = keys[:, head * DK : (head + 1) * DK]
        head_values = values[:, head * DV : (head + 1) * DV]
        spread = jnp.where(causal, running[head, :, None] - running[head, None, :], 0.0)
        decays = jnp.where(causal, jnp.exp(spread), 0.0)
        scores = lax.dot_general(
            head_query, head_keys, (((1,), (1,)), ((), ())), preferred_element_type=jnp.float32
        )
        weights = (scores * decays).astype(jnp.bfloat16)
        outputs.append(
            lax.dot_general(
                weights, head_values, (((1,), (0,)), ((), ())), preferred_element_type=jnp.float32
            )
        )
    return outputs


def make_local(ring_size, copies):
    ring = [(at, (at + 1) % ring_size) for at in range(ring_size)]

    def ring_step(block):
        return lax.ppermute(block, "fs", ring)

    def swap(block, shift):
        return lax.ppermute(
            block, "grp", [(at, (at - shift) % copies) for at in range(copies)]
        )

    def local(
        hidden_activations,
        attention_rescaling_factors,
        feature_rescaling_factors,
        request_matrix,
        request_matrix_multipliers,
        lookup_matrix,
        lookup_matrix_multipliers,
        content_matrix,
        content_matrix_multipliers,
        valve_matrix,
        valve_matrix_multipliers,
        result_matrix,
        result_matrix_multipliers,
        expanding_matrix,
        expand_matrix_multipliers,
        shrinking_matrix,
        shrink_matrix_multipliers,
        attention_fading_logarithm,
        spike_fading_logarithm,
    ):
        fs, grp = lax.axis_index("fs"), lax.axis_index("grp")
        bf16 = jnp.bfloat16

        def owner(hop):
            return (fs - hop) % ring_size

        def part(shift):
            return (grp + shift) % copies

        def chain(shard, axis):
            size = shard.shape[axis] // copies
            pieces = [
                [
                    lax.dynamic_slice_in_dim(shard, part(shift) * size, size, axis).astype(bf16)
                    for shift in range(copies)
                ]
            ]
            block = pieces[0][0]
            for _ in range(1, ring_size):
                block = ring_step(block)
                pieces.append([block] + [swap(block, shift) for shift in range(1, copies)])
            return pieces

        def rows_of(matrix):
            size = matrix.shape[0] // (ring_size * copies)
            return jnp.concatenate(
                [
                    lax.dynamic_slice_in_dim(
                        matrix, (owner(hop) * copies + part(shift)) * size, size, 0
                    )
                    for hop in range(ring_size)
                    for shift in range(copies)
                ],
                axis=0,
            )

        def stack(pieces):
            return jnp.concatenate([piece for hop in pieces for piece in hop], axis=0)

        def columns(pieces):
            rows, size = pieces[0][0].shape
            whole = jnp.zeros((rows, size * ring_size * copies), bf16)
            for hop in range(ring_size):
                for shift in range(copies):
                    start = (owner(hop) * copies + part(shift)) * size
                    whole = lax.dynamic_update_slice(whole, pieces[hop][shift], (0, start))
            return whole

        scales = jnp.stack([result_matrix_multipliers, shrink_matrix_multipliers])
        every_scale = jnp.zeros((2, scales.shape[1] * ring_size), jnp.float32)
        block = scales
        for hop in range(ring_size):
            if hop:
                block = ring_step(block)
            every_scale = lax.dynamic_update_slice(
                every_scale, block, (0, owner(hop) * scales.shape[1])
            )
        out_scales, down_scales = every_scale[0], every_scale[1]

        half_up = expanding_matrix.shape[1] // 2
        half_down = shrinking_matrix.shape[0] // 2
        qk = chain(jnp.concatenate([request_matrix, lookup_matrix], axis=1), 0)
        v = chain(content_matrix, 0)
        gates = chain(valve_matrix, 0)
        out = chain(result_matrix, 1)
        ups = [chain(expanding_matrix[:, :half_up], 0), chain(expanding_matrix[:, half_up:], 0)]
        downs = [chain(shrinking_matrix[:half_down], 1), chain(shrinking_matrix[half_down:], 1)]

        normed = rows_of(
            rms_norm(collect_features(hidden_activations), attention_rescaling_factors)
        )
        width = request_matrix.shape[1]
        qk_sum = project(normed, stack(qk))
        query = (qk_sum[:, :width] * request_matrix_multipliers).astype(bf16)
        keys = (qk_sum[:, width:] * lookup_matrix_multipliers * DK ** (-0.5)).astype(bf16)
        values = (project(normed, stack(v)) * content_matrix_multipliers).astype(bf16)
        rates = attention_fading_logarithm[:, None] + spike_fading_logarithm
        retained = retain(query, keys, values, rates)
        gate = project(normed, stack(gates)) * valve_matrix_multipliers
        heads_out = jnp.concatenate(
            [
                (
                    group_norm(retained[head])
                    * jax.nn.silu(gate[:, head * DV : (head + 1) * DV])
                ).astype(bf16)
                for head in range(len(retained))
            ],
            axis=1,
        )
        update = lax.psum_scatter(
            (
                lax.dot_general(
                    columns(out),
                    heads_out,
                    (((0,), (1,)), ((), ())),
                    preferred_element_type=jnp.float32,
                )
                * out_scales[:, None]
            ).astype(bf16),
            "tp",
            scatter_dimension=0,
            tiled=True,
        ).astype(jnp.float32)
        middle = (hidden_activations.astype(jnp.float32) + update).astype(bf16)
        normed_mlp = rows_of(rms_norm(collect_features(middle), feature_rescaling_factors))
        terms = None
        for side in range(2):
            scale = expand_matrix_multipliers[side * half_up : (side + 1) * half_up]
            rising = jax.nn.relu(project(normed_mlp, stack(ups[side])) * scale)
            hidden = (rising * rising).astype(bf16)
            term = lax.dot_general(
                columns(downs[side]),
                hidden,
                (((0,), (1,)), ((), ())),
                preferred_element_type=jnp.float32,
            )
            terms = term if terms is None else terms + term
        lowered = lax.psum_scatter(
            (terms * down_scales[:, None]).astype(bf16), "tp", scatter_dimension=0, tiled=True
        ).astype(jnp.float32)
        return (middle.astype(jnp.float32) + lowered).astype(bf16)

    return local


def solution(mesh):
    ring_size, copies = mesh.shape["fs"], mesh.shape["grp"]
    placed = (
        P("tp", ("grp", "fs")),
        P(),
        P(),
        P("fs", "tp"),
        P("tp"),
        P("fs", "tp"),
        P("tp"),
        P("fs", "tp"),
        P("tp"),
        P("fs", "tp"),
        P("tp"),
        P("tp", "fs"),
        P("fs"),
        P("fs", "tp"),
        P("tp"),
        P("tp", "fs"),
        P("fs"),
        P("tp"),
        P("tp", ("grp", "fs")),
    )
    return jax.shard_map(
        make_local(ring_size, copies),
        mesh=mesh,
        in_specs=placed,
        out_specs=P("tp", ("grp", "fs")),
        check_vma=False,
    )
```

time: 826 us -> 536 us (0.65)
  waiting for transfers between devices: 651 us -> 326 us
  local copies, waits for them, and re-layouts: 22.6 us -> 78.2 us
  starting transfers between devices: 0.42 us -> 39.9 us
  blocking collectives: 26.4 us -> 0 us
  matrix products: 79.9 us -> 55 us
  other arithmetic: 30.3 us -> 14.1 us
    all_gather x7 -> x0, waiting for transfers between devices: 561 us -> none  [the longest x4 183 us: local(): lax.all_gather(part, 'fs', axis=0, tiled=True)]
    ppermute x0 -> x51, waiting for transfers between devices: none -> 254 us  [the longest x27 154 us: ring_step(): return lax.ppermute(block, 'fs', ring)]
    ppermute x0 -> x51, starting transfers between devices: none -> 39.8 us  [the longest x24 26.3 us: swap(): lax.ppermute(block, 'grp', [(at, (at - shift) % copies) for at in range(c...]
    unnamed x50 -> x100, local copies, waits for them, and re-layouts: 9.17 us -> 37.7 us
    dot_general x20 -> x5, matrix products: 64.1 us -> 36.7 us  [the longest x2 23.7 us: local(): lax.dot_general(columns(downs[side]), hidden, (((0,), (1,)), ((), ())), p...]
    all_gather x2 -> x0, blocking collectives: 26.4 us -> none  [the longest x1 14.3 us: local(): lax.all_gather(result_matrix_multipliers, 'fs', axis=0, tiled=True)]
    dynamic_update_slice x0 -> x27, local copies, waits for them, and re-layouts: none -> 24.9 us  [the longest x24 24.9 us: columns(): whole = lax.dynamic_update_slice(whole, pieces[hop][shift], (0, start))]
    all_gather x2, waiting for transfers between devices: 18.2 us -> 0.01 us  [collect_features(): return lax.all_gather(matrix, 'tp', axis=0, tiled=True)]
  transfers between devices with their start and end apart: 11 -> 55, of which waited for: 11 -> 40; matrix products, arithmetic and copies ran while one was open for 11% -> 13% of each run, Pallas kernels for 0% -> 0%
where the time goes in v1:
time: 536 us; the launch traced here: 528 us
  waiting for transfers between devices  326 us (61%)
  local copies, waits for them, and re-layouts  78.2 us (15%)
  matrix products  55 us (10%)
  starting transfers between devices  39.9 us (7%)
  between operations  14.2 us (3%)
  other arithmetic  14.1 us (3%)
    ppermute x27, waiting for transfers between devices, ring_step(): return lax.ppermute(block, 'fs', ring)  154 us
    ppermute x24, waiting for transfers between devices, swap(): lax.ppermute(block, 'grp', [(at, (at - shift) % copies) for at in range(c...  100 us
    unnamed x100, local copies, waits for them, and re-layouts  37.7 us
    reduce_scatter x1, waiting for transfers between devices, local(): lax.psum_scatter((terms * down_scales[:, None]).astype(bf16), 'tp', scatt...  36.3 us
    reduce_scatter x1, waiting for transfers between devices, local(): lax.psum_scatter((lax.dot_general(columns(out), heads_out, (((0,), (1,)),...  36 us
    ppermute x24, starting transfers between devices, swap(): lax.ppermute(block, 'grp', [(at, (at - shift) % copies) for at in range(c...  26.3 us
    dynamic_update_slice x24, local copies, waits for them, and re-layouts, columns(): whole = lax.dynamic_update_slice(whole, pieces[hop][shift], (0, start))  24.9 us
    dot_general x2, matrix products, local(): lax.dot_general(columns(downs[side]), hidden, (((0,), (1,)), ((), ())), p...  23.7 us
  transfers between devices with their start and end apart: 55, of which 40 were waited for; matrix products, arithmetic and copies ran while one was open for 13% of the time, Pallas kernels for 0%

profile of v1, /device:TPU:0, one launch (start us, length us, event | category | flops | bytes accessed | tf_op | source)
XLA Modules:
  0.0 527.9 jit_solution(7268827547579716232)
XLA Ops:
  10.4 3.1 collective-permute-start.6
  16.3 2.3 constant_dynamic-update-slice_fusion.22
  20.3 2.5 broadcast.90.clone.1
  22.8 2.3 constant_dynamic-update-slice_fusion.61
  25.2 1.8 collective-permute-start.24
  29.7 2.1 fusion.25
  31.8 2.1 fusion.22
  34.0 27.5 %collective-permute-done.24 = f32[2,512]{1,0:T(2,128)S(1)} collective-permute-done((f32[2,512]{1,0:T(2,128)S(1)}, f32[2,512]{1,0:T(2,128)S(1)}, u32[]{:S(2)}, u32[]{:S(2)}) %collective-permute-start.24) | collective-permute-done | bytes 4128 | tf_op jit(solution)/shard_map/ppermute | solution.py:64
  61.5 5.4 %collective-permute-done.25 = f32[2,512]{1,0:T(2,128)S(1)} collective-permute-done((f32[2,512]{1,0:T(2,128)S(1)}, f32[2,512]{1,0:T(2,128)S(1)}, u32[]{:S(2)}, u32[]{:S(2)}) %collective-permute-start.25) | collective-permute-done | bytes 4128 | tf_op jit(solution)/shard_map/ppermute | solution.py:64
  66.9 5.4 %collective-permute-done.26 = f32[2,512]{1,0:T(2,128)S(1)} collective-permute-done((f32[2,512]{1,0:T(2,128)S(1)}, f32[2,512]{1,0:T(2,128)S(1)}, u32[]{:S(2)}, u32[]{:S(2)}) %collective-permute-start.26) | collective-permute-done | bytes 4128 | tf_op jit(solution)/shard_map/ppermute | solution.py:64
  73.9 1.9 constant_dynamic-update-slice_fusion.7
  76.3 2.0 constant_dynamic-update-slice_fusion.14
  78.3 1.9 constant_dynamic-update-slice_fusion.21
  81.7 5.6 %collective-permute-done.7 = bf16[256,1024]{1,0:T(8,128)(2,1)S(1)} collective-permute-done((bf16[256,1024]{1,0:T(8,128)(2,1)}, bf16[256,1024]{1,0:T(8,128)(2,1)S(1)}, u32[]{:S(2)}, u32[]{:S(2)}) %collective-permute-start.7) | collective-permute-done | bytes 524320 | tf_op jit(solution)/shard_map/ppermute | solution.py:67
  87.3 1.9 constant_dynamic-update-slice_fusion.60
  92.5 6.1 %collective-permute-done.13 = bf16[256,1024]{1,0:T(8,128)(2,1)S(1)} collective-permute-done((bf16[256,1024]{1,0:T(8,128)(2,1)}, bf16[256,1024]{1,0:T(8,128)(2,1)S(1)}, u32[]{:S(2)}, u32[]{:S(2)}) %collective-permute-start.13) | collective-permute-done | bytes 524320 | tf_op jit(solution)/shard_map/ppermute | solution.py:67
  98.6 3.4 collective-permute-done.14
  104.1 5.7 %collective-permute-done.19 = bf16[256,1024]{1,0:T(8,128)(2,1)S(1)} collective-permute-done((bf16[256,1024]{1,0:T(8,128)(2,1)}, bf16[256,1024]{1,0:T(8,128)(2,1)S(1)}, u32[]{:S(2)}, u32[]{:S(2)}) %collective-permute-start.19) | collective-permute-done | bytes 524320 | tf_op jit(solution)/shard_map/ppermute | solution.py:67
  109.8 3.4 collective-permute-done.20
  115.3 5.7 %collective-permute-done.1 = bf16[1024,256]{1,0:T(8,128)(2,1)S(1)} collective-permute-done((bf16[1024,256]{1,0:T(8,128)(2,1)}, bf16[1024,256]{1,0:T(8,128)(2,1)S(1)}, u32[]{:S(2)}, u32[]{:S(2)}) %collective-permute-start.1) | collective-permute-done | bytes 524320 | tf_op jit(solution)/shard_map/ppermute | solution.py:67
  121.9 2.5 collective-permute-done.2
  124.9 7.3 %collective-permute-done.9 = bf16[256,1024]{1,0:T(8,128)(2,1)S(1)} collective-permute-done((bf16[256,1024]{1,0:T(8,128)(2,1)S(1)}, bf16[256,1024]{1,0:T(8,128)(2,1)S(1)}, u32[]{:S(2)}, u32[]{:S(2)}) %collective-permute-start.9) | collective-permute-done | bytes 524320 | tf_op jit(solution)/shard_map/ppermute | solution.py:67
  136.2 7.3 %collective-permute-done.15 = bf16[256,1024]{1,0:T(8,128)(2,1)S(1)} collective-permute-done((bf16[256,1024]{1,0:T(8,128)(2,1)S(1)}, bf16[256,1024]{1,0:T(8,128)(2,1)S(1)}, u32[]{:S(2)}, u32[]{:S(2)}) %collective-permute-start.15) | collective-permute-done | bytes 524320 | tf_op jit(solution)/shard_map/ppermute | solution.py:67
  148.3 6.5 %collective-permute-done.21 = bf16[256,1024]{1,0:T(8,128)(2,1)S(1)} collective-permute-done((bf16[256,1024]{1,0:T(8,128)(2,1)S(1)}, bf16[256,1024]{1,0:T(8,128)(2,1)S(1)}, u32[]{:S(2)}, u32[]{:S(2)}) %collective-permute-start.21) | collective-permute-done | bytes 524320 | tf_op jit(solution)/shard_map/ppermute | solution.py:67
  156.3 1.9 collective-permute-done.22
  160.3 4.6 collective-permute-done.4
  167.8 9.4 %collective-permute-done.11 = bf16[256,1024]{1,0:T(8,128)(2,1)S(1)} collective-permute-done((bf16[256,1024]{1,0:T(8,128)(2,1)S(1)}, bf16[256,1024]{1,0:T(8,128)(2,1)S(1)}, u32[]{:S(2)}, u32[]{:S(2)}) %collective-permute-start.11) | collective-permute-done | bytes 524320 | tf_op jit(solution)/shard_map/ppermute | solution.py:67
  178.0 10.4 %collective-permute-done.17 = bf16[256,1024]{1,0:T(8,128)(2,1)S(1)} collective-permute-done((bf16[256,1024]{1,0:T(8,128)(2,1)S(1)}, bf16[256,1024]{1,0:T(8,128)(2,1)S(1)}, u32[]{:S(2)}, u32[]{:S(2)}) %collective-permute-start.17) | collective-permute-done | bytes 524320 | tf_op jit(solution)/shard_map/ppermute | solution.py:67
  189.3 10.3 %collective-permute-done.23 = bf16[256,1024]{1,0:T(8,128)(2,1)S(1)} collective-permute-done((bf16[256,1024]{1,0:T(8,128)(2,1)S(1)}, bf16[256,1024]{1,0:T(8,128)(2,1)S(1)}, u32[]{:S(2)}, u32[]{:S(2)}) %collective-permute-start.23) | collective-permute-done | bytes 524320 | tf_op jit(solution)/shard_map/ppermute | solution.py:67
  200.5 6.4 %collective-permute-done.5 = bf16[1024,256]{1,0:T(8,128)(2,1)S(1)} collective-permute-done((bf16[1024,256]{1,0:T(8,128)(2,1)S(1)}, bf16[1024,256]{1,0:T(8,128)(2,1)S(1)}, u32[]{:S(2)}, u32[]{:S(2)}) %collective-permute-start.5) | collective-permute-done | bytes 524320 | tf_op jit(solution)/shard_map/ppermute | solution.py:67
  207.8 2.7 fusion
  211.8 1.8 copy-done.8
  213.6 3.6 fusion.56
  217.3 4.8 multiply_convert_fusion.4
  222.6 2.9 fusion.46
  225.5 2.6 fusion.51
  228.6 6.3 %convolution_multiply_fusion = f32[768,1024]{0,1:T(8,128)S(1)} fusion(bf16[2048,768]{1,0:T(8,128)(2,1)} %copy-done.13, bf16[2048,1024]{1,0:T(8,128)(2,1)} %constant_dynamic-update-slice_fusion.16, f32[1024]{0:T(1024)S(1)} %copy-done.24), kind=kOutput, calls=%fused_computation.18 | convolution fusion | flops 3222011904 | bytes 10489856 | tf_op jit(solution)/shard_map/dot_general | solution.py:21
  235.8 7.5 %multiply_convert_fusion.1 = bf16[2048,768]{1,0:T(8,128)(2,1)} fusion(bf16[1024,2048]{1,0:T(8,128)(2,1)} %constant_dynamic-update-slice_fusion.55, f32[2048]{0:T(1024)S(1)} %bitcast.24, bf16[768,512]{0,1:T(8,128)(2,1)S(1)} %get-tuple-element.26, bf16[768,512]{0,1:T(8,128)(2,1)S(1)} %get-tuple-element.25), kind=kOutput, calls=%fused_computation.11 | convolution fusion | flops 3227516928 | bytes 8921088 | tf_op jit(solution)/shard_map/dot_general | solution.py:183
  243.4 36.0 %reduce-scatter.3.cloned.1.call-done = bf16[512,768]{1,0:T(8,128)(2,1)} async-done(((bf16[2048,768]{1,0:T(8,128)(2,1)}), bf16[512,768]{1,0:T(8,128)(2,1)}) %reduce-scatter.3.cloned.1.call-update) | async-done | bytes 786448 | tf_op jit(solution)/shard_map/reduce_scatter | solution.py:181
  279.4 2.2 add_convert_fusion.1
  281.7 2.7 fusion.42
  286.3 2.6 broadcast.90.clone
  291.3 2.5 broadcast.90.clone.2
  298.5 2.6 collective-permute-done.45
  304.4 8.0 %collective-permute-done.39 = bf16[1024,256]{1,0:T(8,128)(2,1)S(1)} collective-permute-done((bf16[1024,256]{1,0:T(8,128)(2,1)S(1)}, bf16[1024,256]{1,0:T(8,128)(2,1)S(1)}, u32[]{:S(2)}, u32[]{:S(2)}) %collective-permute-start.39) | collective-permute-done | bytes 524320 | tf_op jit(solution)/shard_map/ppermute | solution.py:64
  313.9 9.8 %collective-permute-done.27 = bf16[1024,256]{1,0:T(8,128)(2,1)S(1)} collective-permute-done((bf16[1024,256]{1,0:T(8,128)(2,1)S(1)}, bf16[1024,256]{1,0:T(8,128)(2,1)S(1)}, u32[]{:S(2)}, u32[]{:S(2)}) %collective-permute-start.27) | collective-permute-done | bytes 524320 | tf_op jit(solution)/shard_map/ppermute | solution.py:64
  325.4 9.5 %collective-permute-done.33 = bf16[256,1024]{1,0:T(8,128)(2,1)S(1)} collective-permute-done((bf16[256,1024]{1,0:T(8,128)(2,1)S(1)}, bf16[256,1024]{1,0:T(8,128)(2,1)S(1)}, u32[]{:S(2)}, u32[]{:S(2)}) %collective-permute-start.33) | collective-permute-done | bytes 524320 | tf_op jit(solution)/shard_map/ppermute | solution.py:64
  337.3 8.9 %collective-permute-done.47 = bf16[256,1024]{1,0:T(8,128)(2,1)S(1)} collective-permute-done((bf16[256,1024]{1,0:T(8,128)(2,1)S(1)}, bf16[256,1024]{1,0:T(8,128)(2,1)S(1)}, u32[]{:S(2)}, u32[]{:S(2)}) %collective-permute-start.47) | collective-permute-done | bytes 524320 | tf_op jit(solution)/shard_map/ppermute | solution.py:64
  347.7 9.7 %collective-permute-done.41 = bf16[1024,256]{1,0:T(8,128)(2,1)S(1)} collective-permute-done((bf16[1024,256]{1,0:T(8,128)(2,1)S(1)}, bf16[1024,256]{1,0:T(8,128)(2,1)S(1)}, u32[]{:S(2)}, u32[]{:S(2)}) %collective-permute-start.41) | collective-permute-done | bytes 524320 | tf_op jit(solution)/shard_map/ppermute | solution.py:64
  360.6 8.0 %collective-permute-done.29 = bf16[1024,256]{1,0:T(8,128)(2,1)S(1)} collective-permute-done((bf16[1024,256]{1,0:T(8,128)(2,1)S(1)}, bf16[1024,256]{1,0:T(8,128)(2,1)S(1)}, u32[]{:S(2)}, u32[]{:S(2)}) %collective-permute-start.29) | collective-permute-done | bytes 524320 | tf_op jit(solution)/shard_map/ppermute | solution.py:64
  372.7 7.1 %collective-permute-done.35 = bf16[256,1024]{1,0:T(8,128)(2,1)S(1)} collective-permute-done((bf16[256,1024]{1,0:T(8,128)(2,1)S(1)}, bf16[256,1024]{1,0:T(8,128)(2,1)S(1)}, u32[]{:S(2)}, u32[]{:S(2)}) %collective-permute-start.35) | collective-permute-done | bytes 524320 | tf_op jit(solution)/shard_map/ppermute | solution.py:64
  382.2 8.9 %collective-permute-done.49 = bf16[256,1024]{1,0:T(8,128)(2,1)S(1)} collective-permute-done((bf16[256,1024]{1,0:T(8,128)(2,1)S(1)}, bf16[256,1024]{1,0:T(8,128)(2,1)S(1)}, u32[]{:S(2)}, u32[]{:S(2)}) %collective-permute-start.49) | collective-permute-done | bytes 524320 | tf_op jit(solution)/shard_map/ppermute | solution.py:64
  393.6 8.6 %collective-permute-done.43 = bf16[1024,256]{1,0:T(8,128)(2,1)S(1)} collective-permute-done((bf16[1024,256]{1,0:T(8,128)(2,1)S(1)}, bf16[1024,256]{1,0:T(8,128)(2,1)S(1)}, u32[]{:S(2)}, u32[]{:S(2)}) %collective-permute-start.43) | collective-permute-done | bytes 524320 | tf_op jit(solution)/shard_map/ppermute | solution.py:64
  405.2 8.3 %collective-permute-done.31 = bf16[1024,256]{1,0:T(8,128)(2,1)S(1)} collective-permute-done((bf16[1024,256]{1,0:T(8,128)(2,1)S(1)}, bf16[1024,256]{1,0:T(8,128)(2,1)S(1)}, u32[]{:S(2)}, u32[]{:S(2)}) %collective-permute-start.31) | collective-permute-done | bytes 524320 | tf_op jit(solution)/shard_map/ppermute | solution.py:64
  416.7 6.7 %collective-permute-done.37 = bf16[256,1024]{1,0:T(8,128)(2,1)S(1)} collective-permute-done((bf16[256,1024]{1,0:T(8,128)(2,1)S(1)}, bf16[256,1024]{1,0:T(8,128)(2,1)S(1)}, u32[]{:S(2)}, u32[]{:S(2)}) %collective-permute-start.37) | collective-permute-done | bytes 524320 | tf_op jit(solution)/shard_map/ppermute | solution.py:64
  429.2 10.3 %collective-permute-done.32 = bf16[1024,256]{1,0:T(8,128)(2,1)S(1)} collective-permute-done((bf16[1024,256]{1,0:T(8,128)(2,1)S(1)}, bf16[1024,256]{1,0:T(8,128)(2,1)S(1)}, u32[]{:S(2)}, u32[]{:S(2)}) %collective-permute-start.32) | collective-permute-done | bytes 524320 | tf_op jit(solution)/shard_map/ppermute | solution.py:67
  440.4 6.9 %collective-permute-done.38 = bf16[256,1024]{1,0:T(8,128)(2,1)S(1)} collective-permute-done((bf16[256,1024]{1,0:T(8,128)(2,1)S(1)}, bf16[256,1024]{1,0:T(8,128)(2,1)S(1)}, u32[]{:S(2)}, u32[]{:S(2)}) %collective-permute-start.38) | collective-permute-done | bytes 524320 | tf_op jit(solution)/shard_map/ppermute | solution.py:67
  448.1 2.7 fusion.3
  452.1 3.0 copy-done.11
  455.1 3.6 multiply_convert_fusion.2
  458.7 8.4 %fusion.57 = f32[2048,768]{1,0:T(8,128)} fusion(bf16[1024,2048]{1,0:T(8,128)(2,1)} %constant_dynamic-update-slice_fusion.42, bf16[768,1024]{1,0:T(8,128)(2,1)S(1)} %multiply_convert_fusion.2), kind=kOutput, calls=%fused_computation.172 | convolution fusion | flops 3221225472 | bytes 12058624 | tf_op jit(solution)/shard_map/dot_general | solution.py:202
  467.2 15.3 %multiply_convert_fusion = bf16[2048,768]{1,0:T(8,128)(2,1)} fusion(f32[2048,768]{1,0:T(8,128)} %fusion.57, bf16[1024,2048]{1,0:T(8,128)(2,1)} %constant_dynamic-update-slice_fusion.44, f32[2048]{0:T(1024)S(1)} %bitcast.23, bf16[2048,768]{1,0:T(8,128)(2,1)} %copy-done.12, bf16[2048,1024]{1,0:T(8,128)(2,1)} %constant_dynamic-update-slice_fusion.23, ...), kind=kOutput, calls=%fused_computation.10 | convolution fusion | flops 6450315264 | bytes 20983808 | tf_op jit(solution)/shard_map/dot_general | solution.py:202
  482.5 36.3 %reduce-scatter.5.cloned.1.call-done = bf16[512,768]{1,0:T(8,128)(2,1)} async-done(((bf16[2048,768]{1,0:T(8,128)(2,1)}), bf16[512,768]{1,0:T(8,128)(2,1)}) %reduce-scatter.5.cloned.1.call-update) | async-done | bytes 786448 | tf_op jit(solution)/shard_map/reduce_scatter | solution.py:209
  518.7 2.2 add_convert_fusion
  (225 shorter events, 92.0 us)
Async XLA Ops:
  6.5 201.3 %all-gather.3.cloned.1.call-start = ((), (), s32[]{:S(2)}) async-start(), calls=%async_computation.2 | async-start | bytes 3932160 | tf_op jit(solution)/shard_map/all_gather | solution.py:27
  10.4 61.9 %collective-permute-start.6 = (bf16[256,1024]{1,0:T(8,128)(2,1)}, bf16[256,1024]{1,0:T(8,128)(2,1)}, u32[]{:S(2)}, u32[]{:S(2)}) collective-permute-start(bf16[256,1024]{1,0:T(8,128)(2,1)} %get-tuple-element.12), channel_id=1, source_target_pairs={{0,4},{4,8},{8,12},{12,0},{1,5},{5,9},{9,13},{13,1},{2,6},{6,10},{... | collective-permute-start | bytes 1572872 | tf_op jit(solution)/shard_map/ppermute | solution.py:64
  13.5 11.6 %copy-start.20 = (f32[512]{0:T(512)S(1)}, f32[512]{0:T(512)}, u32[]{:S(2)}) copy-start(f32[512]{0:T(512)} %param.35) | copy-start | bytes 6148
  13.5 11.6 %copy-start.21 = (f32[512]{0:T(512)S(1)}, f32[512]{0:T(512)}, u32[]{:S(2)}) copy-start(f32[512]{0:T(512)} %param.31) | copy-start | bytes 6148
  13.5 13.5 %copy-start.17 = (f32[2,768]{1,0:T(2,128)S(1)}, f32[2,768]{1,0:T(2,128)}, u32[]{:S(2)}) copy-start(f32[2,768]{1,0:T(2,128)} %param.37) | copy-start | bytes 18436
  13.5 13.5 %copy-start.22 = (f32[2]{0:T(128)S(1)}, f32[2]{0:T(128)}, u32[]{:S(2)}) copy-start(f32[2]{0:T(128)} %param.36) | copy-start | bytes 28
  13.6 265.8 %reduce-scatter.3.cloned.1.call-start = ((), (), s32[]{:S(2)}) async-start(), calls=%async_computation.3 | async-start | bytes 3932160 | tf_op jit(solution)/shard_map/reduce_scatter | solution.py:181
  14.8 61.1 %collective-permute-start.12 = (bf16[256,1024]{1,0:T(8,128)(2,1)}, bf16[256,1024]{1,0:T(8,128)(2,1)}, u32[]{:S(2)}, u32[]{:S(2)}) collective-permute-start(bf16[256,1024]{1,0:T(8,128)(2,1)} %get-tuple-element.14), channel_id=1, source_target_pairs={{0,4},{4,8},{8,12},{12,0},{1,5},{5,9},{9,13},{13,1},{2,6},{6,10},{... | collective-permute-start | bytes 1572872 | tf_op jit(solution)/shard_map/ppermute | solution.py:64
  18.7 57.7 %collective-permute-start.18 = (bf16[256,1024]{1,0:T(8,128)(2,1)}, bf16[256,1024]{1,0:T(8,128)(2,1)}, u32[]{:S(2)}, u32[]{:S(2)}) collective-permute-start(bf16[256,1024]{1,0:T(8,128)(2,1)} %get-tuple-element.16), channel_id=1, source_target_pairs={{0,4},{4,8},{8,12},{12,0},{1,5},{5,9},{9,13},{13,1},{2,6},{6,10},{... | collective-permute-start | bytes 1572872 | tf_op jit(solution)/shard_map/ppermute | solution.py:64
  25.1 55.1 %collective-permute-start = (bf16[1024,256]{1,0:T(8,128)(2,1)}, bf16[1024,256]{1,0:T(8,128)(2,1)}, u32[]{:S(2)}, u32[]{:S(2)}) collective-permute-start(bf16[1024,256]{1,0:T(8,128)(2,1)} %get-tuple-element.18), channel_id=1, source_target_pairs={{0,4},{4,8},{8,12},{12,0},{1,5},{5,9},{9,13},{13,1},{2,6},{6,10},{... | collective-permute-start | bytes 1572872 | tf_op jit(solution)/shard_map/ppermute | solution.py:64
  25.2 36.3 %collective-permute-start.24 = (f32[2,512]{1,0:T(2,128)S(1)}, f32[2,512]{1,0:T(2,128)S(1)}, u32[]{:S(2)}, u32[]{:S(2)}) collective-permute-start(f32[2,512]{1,0:T(2,128)S(1)} %get-tuple-element.35), channel_id=1, source_target_pairs={{0,4},{4,8},{8,12},{12,0},{1,5},{5,9},{9,13},{13,1},{2,6},{6,10},{... | collective-permute-start | bytes 12296 | tf_op jit(solution)/shard_map/ppermute | solution.py:64
  61.5 5.4 %collective-permute-start.25 = (f32[2,512]{1,0:T(2,128)S(1)}, f32[2,512]{1,0:T(2,128)S(1)}, u32[]{:S(2)}, u32[]{:S(2)}) collective-permute-start(f32[2,512]{1,0:T(2,128)S(1)} %collective-permute-done.24), channel_id=1, source_target_pairs={{0,4},{4,8},{8,12},{12,0},{1,5},{5,9},{9,13},{13,1},{2,6},{6,10},{... | collective-permute-start | bytes 12296 | tf_op jit(solution)/shard_map/ppermute | solution.py:64
  66.9 5.4 %collective-permute-start.26 = (f32[2,512]{1,0:T(2,128)S(1)}, f32[2,512]{1,0:T(2,128)S(1)}, u32[]{:S(2)}, u32[]{:S(2)}) collective-permute-start(f32[2,512]{1,0:T(2,128)S(1)} %collective-permute-done.25), channel_id=1, source_target_pairs={{0,4},{4,8},{8,12},{12,0},{1,5},{5,9},{9,13},{13,1},{2,6},{6,10},{... | collective-permute-start | bytes 12296 | tf_op jit(solution)/shard_map/ppermute | solution.py:64
  72.3 15.0 %collective-permute-start.7 = (bf16[256,1024]{1,0:T(8,128)(2,1)}, bf16[256,1024]{1,0:T(8,128)(2,1)S(1)}, u32[]{:S(2)}, u32[]{:S(2)}) collective-permute-start(bf16[256,1024]{1,0:T(8,128)(2,1)} %collective-permute-done.6), channel_id=1, source_target_pairs={{0,16},{16,0},{1,17},{17,1},{2,18},{18,2},{3,19},{19,3},{4,20},{20... | collective-permute-start | bytes 1572872 | tf_op jit(solution)/shard_map/ppermute | solution.py:67
  73.9 16.9 %collective-permute-start.8 = (bf16[256,1024]{1,0:T(8,128)(2,1)}, bf16[256,1024]{1,0:T(8,128)(2,1)S(1)}, u32[]{:S(2)}, u32[]{:S(2)}) collective-permute-start(bf16[256,1024]{1,0:T(8,128)(2,1)} %collective-permute-done.6), channel_id=1, source_target_pairs={{0,4},{4,8},{8,12},{12,0},{1,5},{5,9},{9,13},{13,1},{2,6},{6,10},{... | collective-permute-start | bytes 1572872 | tf_op jit(solution)/shard_map/ppermute | solution.py:64
  75.8 22.7 %collective-permute-start.13 = (bf16[256,1024]{1,0:T(8,128)(2,1)}, bf16[256,1024]{1,0:T(8,128)(2,1)S(1)}, u32[]{:S(2)}, u32[]{:S(2)}) collective-permute-start(bf16[256,1024]{1,0:T(8,128)(2,1)} %collective-permute-done.12), channel_id=1, source_target_pairs={{0,16},{16,0},{1,17},{17,1},{2,18},{18,2},{3,19},{19,3},{4,20},{20... | collective-permute-start | bytes 1572872 | tf_op jit(solution)/shard_map/ppermute | solution.py:67
  76.3 25.6 %collective-permute-start.14 = (bf16[256,1024]{1,0:T(8,128)(2,1)}, bf16[256,1024]{1,0:T(8,128)(2,1)S(1)}, u32[]{:S(2)}, u32[]{:S(2)}) collective-permute-start(bf16[256,1024]{1,0:T(8,128)(2,1)} %collective-permute-done.12), channel_id=1, source_target_pairs={{0,4},{4,8},{8,12},{12,0},{1,5},{5,9},{9,13},{13,1},{2,6},{6,10},{... | collective-permute-start | bytes 1572872 | tf_op jit(solution)/shard_map/ppermute | solution.py:64
  80.2 29.6 %collective-permute-start.19 = (bf16[256,1024]{1,0:T(8,128)(2,1)}, bf16[256,1024]{1,0:T(8,128)(2,1)S(1)}, u32[]{:S(2)}, u32[]{:S(2)}) collective-permute-start(bf16[256,1024]{1,0:T(8,128)(2,1)} %collective-permute-done.18), channel_id=1, source_target_pairs={{0,16},{16,0},{1,17},{17,1},{2,18},{18,2},{3,19},{19,3},{4,20},{20... | collective-permute-start | bytes 1572872 | tf_op jit(solution)/shard_map/ppermute | solution.py:67
  87.3 25.9 %collective-permute-start.20 = (bf16[256,1024]{1,0:T(8,128)(2,1)}, bf16[256,1024]{1,0:T(8,128)(2,1)S(1)}, u32[]{:S(2)}, u32[]{:S(2)}) collective-permute-start(bf16[256,1024]{1,0:T(8,128)(2,1)} %collective-permute-done.18), channel_id=1, source_target_pairs={{0,4},{4,8},{8,12},{12,0},{1,5},{5,9},{9,13},{13,1},{2,6},{6,10},{... | collective-permute-start | bytes 1572872 | tf_op jit(solution)/shard_map/ppermute | solution.py:64
  90.7 30.3 %collective-permute-start.1 = (bf16[1024,256]{1,0:T(8,128)(2,1)}, bf16[1024,256]{1,0:T(8,128)(2,1)S(1)}, u32[]{:S(2)}, u32[]{:S(2)}) collective-permute-start(bf16[1024,256]{1,0:T(8,128)(2,1)} %collective-permute-done), channel_id=1, source_target_pairs={{0,16},{16,0},{1,17},{17,1},{2,18},{18,2},{3,19},{19,3},{4,20},{20... | collective-permute-start | bytes 1572872 | tf_op jit(solution)/shard_map/ppermute | solution.py:67
  98.6 25.9 %collective-permute-start.2 = (bf16[1024,256]{1,0:T(8,128)(2,1)}, bf16[1024,256]{1,0:T(8,128)(2,1)S(1)}, u32[]{:S(2)}, u32[]{:S(2)}) collective-permute-start(bf16[1024,256]{1,0:T(8,128)(2,1)} %collective-permute-done), channel_id=1, source_target_pairs={{0,4},{4,8},{8,12},{12,0},{1,5},{5,9},{9,13},{13,1},{2,6},{6,10},{... | collective-permute-start | bytes 1572872 | tf_op jit(solution)/shard_map/ppermute | solution.py:64
  101.9 30.3 %collective-permute-start.9 = (bf16[256,1024]{1,0:T(8,128)(2,1)S(1)}, bf16[256,1024]{1,0:T(8,128)(2,1)S(1)}, u32[]{:S(2)}, u32[]{:S(2)}) collective-permute-start(bf16[256,1024]{1,0:T(8,128)(2,1)S(1)} %collective-permute-done.8), channel_id=1, source_target_pairs={{0,16},{16,0},{1,17},{17,1},{2,18},{18,2},{3,19},{19,3},{4,20},{20... | collective-permute-start | bytes 1572872 | tf_op jit(solution)/shard_map/ppermute | solution.py:67
  109.8 25.9 %collective-permute-start.10 = (bf16[256,1024]{1,0:T(8,128)(2,1)S(1)}, bf16[256,1024]{1,0:T(8,128)(2,1)S(1)}, u32[]{:S(2)}, u32[]{:S(2)}) collective-permute-start(bf16[256,1024]{1,0:T(8,128)(2,1)S(1)} %collective-permute-done.8), channel_id=1, source_target_pairs={{0,4},{4,8},{8,12},{12,0},{1,5},{5,9},{9,13},{13,1},{2,6},{6,10},{... | collective-permute-start | bytes 1572872 | tf_op jit(solution)/shard_map/ppermute | solution.py:64
  113.2 30.3 %collective-permute-start.15 = (bf16[256,1024]{1,0:T(8,128)(2,1)S(1)}, bf16[256,1024]{1,0:T(8,128)(2,1)S(1)}, u32[]{:S(2)}, u32[]{:S(2)}) collective-permute-start(bf16[256,1024]{1,0:T(8,128)(2,1)S(1)} %collective-permute-done.14), channel_id=1, source_target_pairs={{0,16},{16,0},{1,17},{17,1},{2,18},{18,2},{3,19},{19,3},{4,20},{20... | collective-permute-start | bytes 1572872 | tf_op jit(solution)/shard_map/ppermute | solution.py:67
  121.0 25.9 %collective-permute-start.16 = (bf16[256,1024]{1,0:T(8,128)(2,1)S(1)}, bf16[256,1024]{1,0:T(8,128)(2,1)S(1)}, u32[]{:S(2)}, u32[]{:S(2)}) collective-permute-start(bf16[256,1024]{1,0:T(8,128)(2,1)S(1)} %collective-permute-done.14), channel_id=1, source_target_pairs={{0,4},{4,8},{8,12},{12,0},{1,5},{5,9},{9,13},{13,1},{2,6},{6,10},{... | collective-permute-start | bytes 1572872 | tf_op jit(solution)/shard_map/ppermute | solution.py:64
  124.4 30.3 %collective-permute-start.21 = (bf16[256,1024]{1,0:T(8,128)(2,1)S(1)}, bf16[256,1024]{1,0:T(8,128)(2,1)S(1)}, u32[]{:S(2)}, u32[]{:S(2)}) collective-permute-start(bf16[256,1024]{1,0:T(8,128)(2,1)S(1)} %collective-permute-done.20), channel_id=1, source_target_pairs={{0,16},{16,0},{1,17},{17,1},{2,18},{18,2},{3,19},{19,3},{4,20},{20... | collective-permute-start | bytes 1572872 | tf_op jit(solution)/shard_map/ppermute | solution.py:67
  132.3 25.9 %collective-permute-start.22 = (bf16[256,1024]{1,0:T(8,128)(2,1)S(1)}, bf16[256,1024]{1,0:T(8,128)(2,1)S(1)}, u32[]{:S(2)}, u32[]{:S(2)}) collective-permute-start(bf16[256,1024]{1,0:T(8,128)(2,1)S(1)} %collective-permute-done.20), channel_id=1, source_target_pairs={{0,4},{4,8},{8,12},{12,0},{1,5},{5,9},{9,13},{13,1},{2,6},{6,10},{... | collective-permute-start | bytes 1572872 | tf_op jit(solution)/shard_map/ppermute | solution.py:64
  135.7 30.3 %collective-permute-start.3 = (bf16[1024,256]{1,0:T(8,128)(2,1)S(1)}, bf16[1024,256]{1,0:T(8,128)(2,1)S(1)}, u32[]{:S(2)}, u32[]{:S(2)}) collective-permute-start(bf16[1024,256]{1,0:T(8,128)(2,1)S(1)} %collective-permute-done.2), channel_id=1, source_target_pairs={{0,16},{16,0},{1,17},{17,1},{2,18},{18,2},{3,19},{19,3},{4,20},{20... | collective-permute-start | bytes 1572872 | tf_op jit(solution)/shard_map/ppermute | solution.py:67
  143.5 21.4 %collective-permute-start.4 = (bf16[1024,256]{1,0:T(8,128)(2,1)S(1)}, bf16[1024,256]{1,0:T(8,128)(2,1)S(1)}, u32[]{:S(2)}, u32[]{:S(2)}) collective-permute-start(bf16[1024,256]{1,0:T(8,128)(2,1)S(1)} %collective-permute-done.2), channel_id=1, source_target_pairs={{0,4},{4,8},{8,12},{12,0},{1,5},{5,9},{9,13},{13,1},{2,6},{6,10},{... | collective-permute-start | bytes 1572872 | tf_op jit(solution)/shard_map/ppermute | solution.py:64
  146.9 30.3 %collective-permute-start.11 = (bf16[256,1024]{1,0:T(8,128)(2,1)S(1)}, bf16[256,1024]{1,0:T(8,128)(2,1)S(1)}, u32[]{:S(2)}, u32[]{:S(2)}) collective-permute-start(bf16[256,1024]{1,0:T(8,128)(2,1)S(1)} %collective-permute-done.10), channel_id=1, source_target_pairs={{0,16},{16,0},{1,17},{17,1},{2,18},{18,2},{3,19},{19,3},{4,20},{20... | collective-permute-start | bytes 1572872 | tf_op jit(solution)/shard_map/ppermute | solution.py:67
  154.7 33.7 %collective-permute-start.17 = (bf16[256,1024]{1,0:T(8,128)(2,1)S(1)}, bf16[256,1024]{1,0:T(8,128)(2,1)S(1)}, u32[]{:S(2)}, u32[]{:S(2)}) collective-permute-start(bf16[256,1024]{1,0:T(8,128)(2,1)S(1)} %collective-permute-done.16), channel_id=1, source_target_pairs={{0,16},{16,0},{1,17},{17,1},{2,18},{18,2},{3,19},{19,3},{4,20},{20... | collective-permute-start | bytes 1572872 | tf_op jit(solution)/shard_map/ppermute | solution.py:67
  158.1 41.6 %collective-permute-start.23 = (bf16[256,1024]{1,0:T(8,128)(2,1)S(1)}, bf16[256,1024]{1,0:T(8,128)(2,1)S(1)}, u32[]{:S(2)}, u32[]{:S(2)}) collective-permute-start(bf16[256,1024]{1,0:T(8,128)(2,1)S(1)} %collective-permute-done.22), channel_id=1, source_target_pairs={{0,16},{16,0},{1,17},{17,1},{2,18},{18,2},{3,19},{19,3},{4,20},{20... | collective-permute-start | bytes 1572872 | tf_op jit(solution)/shard_map/ppermute | solution.py:67
  164.9 42.1 %collective-permute-start.5 = (bf16[1024,256]{1,0:T(8,128)(2,1)S(1)}, bf16[1024,256]{1,0:T(8,128)(2,1)S(1)}, u32[]{:S(2)}, u32[]{:S(2)}) collective-permute-start(bf16[1024,256]{1,0:T(8,128)(2,1)S(1)} %collective-permute-done.4), channel_id=1, source_target_pairs={{0,16},{16,0},{1,17},{17,1},{2,18},{18,2},{3,19},{19,3},{4,20},{20... | collective-permute-start | bytes 1572872 | tf_op jit(solution)/shard_map/ppermute | solution.py:67
  166.9 43.7 %copy-start.14 = (f32[2048]{0:T(1024)S(1)}, f32[2048]{0:T(1024)}, u32[]{:S(2)}) copy-start(f32[2048]{0:T(1024)} %param.20) | copy-start | bytes 24580
  235.8 43.6 %copy-start.3 = (bf16[512,768]{1,0:T(8,128)(2,1)S(1)}, bf16[512,768]{1,0:T(8,128)(2,1)}, u32[]{:S(2)}) copy-start(bf16[512,768]{1,0:T(8,128)(2,1)} %param.19) | copy-start | bytes 2359300
  243.3 204.8 %all-gather.5.cloned.1.call-start = ((), (), s32[]{:S(2)}) async-start(), calls=%async_computation.4 | async-start | bytes 3932160 | tf_op jit(solution)/shard_map/all_gather | solution.py:27
  281.6 237.1 %reduce-scatter.5.cloned.1.call-start = ((), (), s32[]{:S(2)}) async-start(), calls=%async_computation.5 | async-start | bytes 3932160 | tf_op jit(solution)/shard_map/reduce_scatter | solution.py:209
  284.5 16.6 %collective-permute-start.45 = (bf16[256,1024]{1,0:T(8,128)(2,1)S(1)}, bf16[256,1024]{1,0:T(8,128)(2,1)S(1)}, u32[]{:S(2)}, u32[]{:S(2)}) collective-permute-start(bf16[256,1024]{1,0:T(8,128)(2,1)S(1)} %get-tuple-element.10), channel_id=1, source_target_pairs={{0,4},{4,8},{8,12},{12,0},{1,5},{5,9},{9,13},{13,1},{2,6},{6,10},{... | collective-permute-start | bytes 1572872 | tf_op jit(solution)/shard_map/ppermute | solution.py:64
  289.8 22.6 %collective-permute-start.39 = (bf16[1024,256]{1,0:T(8,128)(2,1)S(1)}, bf16[1024,256]{1,0:T(8,128)(2,1)S(1)}, u32[]{:S(2)}, u32[]{:S(2)}) collective-permute-start(bf16[1024,256]{1,0:T(8,128)(2,1)S(1)} %get-tuple-element.20), channel_id=1, source_target_pairs={{0,4},{4,8},{8,12},{12,0},{1,5},{5,9},{9,13},{13,1},{2,6},{6,10},{... | collective-permute-start | bytes 1572872 | tf_op jit(solution)/shard_map/ppermute | solution.py:64
  294.7 29.0 %collective-permute-start.27 = (bf16[1024,256]{1,0:T(8,128)(2,1)S(1)}, bf16[1024,256]{1,0:T(8,128)(2,1)S(1)}, u32[]{:S(2)}, u32[]{:S(2)}) collective-permute-start(bf16[1024,256]{1,0:T(8,128)(2,1)S(1)} %get-tuple-element.8), channel_id=1, source_target_pairs={{0,4},{4,8},{8,12},{12,0},{1,5},{5,9},{9,13},{13,1},{2,6},{6,10},{... | collective-permute-start | bytes 1572872 | tf_op jit(solution)/shard_map/ppermute | solution.py:64
  297.1 37.8 %collective-permute-start.33 = (bf16[256,1024]{1,0:T(8,128)(2,1)S(1)}, bf16[256,1024]{1,0:T(8,128)(2,1)S(1)}, u32[]{:S(2)}, u32[]{:S(2)}) collective-permute-start(bf16[256,1024]{1,0:T(8,128)(2,1)S(1)} %get-tuple-element.6), channel_id=1, source_target_pairs={{0,4},{4,8},{8,12},{12,0},{1,5},{5,9},{9,13},{13,1},{2,6},{6,10},{... | collective-permute-start | bytes 1572872 | tf_op jit(solution)/shard_map/ppermute | solution.py:64
  301.2 35.2 %collective-permute-start.46 = (bf16[256,1024]{1,0:T(8,128)(2,1)S(1)}, bf16[256,1024]{1,0:T(8,128)(2,1)S(1)}, u32[]{:S(2)}, u32[]{:S(2)}) collective-permute-start(bf16[256,1024]{1,0:T(8,128)(2,1)S(1)} %collective-permute-done.45), channel_id=1, source_target_pairs={{0,16},{16,0},{1,17},{17,1},{2,18},{18,2},{3,19},{19,3},{4,20},{20... | collective-permute-start | bytes 1572872 | tf_op jit(solution)/shard_map/ppermute | solution.py:67
  304.4 41.7 %collective-permute-start.47 = (bf16[256,1024]{1,0:T(8,128)(2,1)S(1)}, bf16[256,1024]{1,0:T(8,128)(2,1)S(1)}, u32[]{:S(2)}, u32[]{:S(2)}) collective-permute-start(bf16[256,1024]{1,0:T(8,128)(2,1)S(1)} %collective-permute-done.45), channel_id=1, source_target_pairs={{0,4},{4,8},{8,12},{12,0},{1,5},{5,9},{9,13},{13,1},{2,6},{6,10},{... | collective-permute-start | bytes 1572872 | tf_op jit(solution)/shard_map/ppermute | solution.py:64
  312.4 35.2 %collective-permute-start.40 = (bf16[1024,256]{1,0:T(8,128)(2,1)S(1)}, bf16[1024,256]{1,0:T(8,128)(2,1)S(1)}, u32[]{:S(2)}, u32[]{:S(2)}) collective-permute-start(bf16[1024,256]{1,0:T(8,128)(2,1)S(1)} %collective-permute-done.39), channel_id=1, source_target_pairs={{0,16},{16,0},{1,17},{17,1},{2,18},{18,2},{3,19},{19,3},{4,20},{20... | collective-permute-start | bytes 1572872 | tf_op jit(solution)/shard_map/ppermute | solution.py:67
  323.6 33.7 %collective-permute-start.41 = (bf16[1024,256]{1,0:T(8,128)(2,1)S(1)}, bf16[1024,256]{1,0:T(8,128)(2,1)S(1)}, u32[]{:S(2)}, u32[]{:S(2)}) collective-permute-start(bf16[1024,256]{1,0:T(8,128)(2,1)S(1)} %collective-permute-done.39), channel_id=1, source_target_pairs={{0,4},{4,8},{8,12},{12,0},{1,5},{5,9},{9,13},{13,1},{2,6},{6,10},{... | collective-permute-start | bytes 1572872 | tf_op jit(solution)/shard_map/ppermute | solution.py:64
  334.9 25.7 %collective-permute-start.28 = (bf16[1024,256]{1,0:T(8,128)(2,1)S(1)}, bf16[1024,256]{1,0:T(8,128)(2,1)S(1)}, u32[]{:S(2)}, u32[]{:S(2)}) collective-permute-start(bf16[1024,256]{1,0:T(8,128)(2,1)S(1)} %collective-permute-done.27), channel_id=1, source_target_pairs={{0,16},{16,0},{1,17},{17,1},{2,18},{18,2},{3,19},{19,3},{4,20},{20... | collective-permute-start | bytes 1572872 | tf_op jit(solution)/shard_map/ppermute | solution.py:67
  336.3 32.3 %collective-permute-start.29 = (bf16[1024,256]{1,0:T(8,128)(2,1)S(1)}, bf16[1024,256]{1,0:T(8,128)(2,1)S(1)}, u32[]{:S(2)}, u32[]{:S(2)}) collective-permute-start(bf16[1024,256]{1,0:T(8,128)(2,1)S(1)} %collective-permute-done.27), channel_id=1, source_target_pairs={{0,4},{4,8},{8,12},{12,0},{1,5},{5,9},{9,13},{13,1},{2,6},{6,10},{... | collective-permute-start | bytes 1572872 | tf_op jit(solution)/shard_map/ppermute | solution.py:64
  346.1 25.7 %collective-permute-start.34 = (bf16[256,1024]{1,0:T(8,128)(2,1)S(1)}, bf16[256,1024]{1,0:T(8,128)(2,1)S(1)}, u32[]{:S(2)}, u32[]{:S(2)}) collective-permute-start(bf16[256,1024]{1,0:T(8,128)(2,1)S(1)} %collective-permute-done.33), channel_id=1, source_target_pairs={{0,16},{16,0},{1,17},{17,1},{2,18},{18,2},{3,19},{19,3},{4,20},{20... | collective-permute-start | bytes 1572872 | tf_op jit(solution)/shard_map/ppermute | solution.py:67
  347.6 32.2 %collective-permute-start.35 = (bf16[256,1024]{1,0:T(8,128)(2,1)S(1)}, bf16[256,1024]{1,0:T(8,128)(2,1)S(1)}, u32[]{:S(2)}, u32[]{:S(2)}) collective-permute-start(bf16[256,1024]{1,0:T(8,128)(2,1)S(1)} %collective-permute-done.33), channel_id=1, source_target_pairs={{0,4},{4,8},{8,12},{12,0},{1,5},{5,9},{9,13},{13,1},{2,6},{6,10},{... | collective-permute-start | bytes 1572872 | tf_op jit(solution)/shard_map/ppermute | solution.py:64
  357.4 23.9 %collective-permute-start.48 = (bf16[256,1024]{1,0:T(8,128)(2,1)S(1)}, bf16[256,1024]{1,0:T(8,128)(2,1)S(1)}, u32[]{:S(2)}, u32[]{:S(2)}) collective-permute-start(bf16[256,1024]{1,0:T(8,128)(2,1)S(1)} %collective-permute-done.47), channel_id=1, source_target_pairs={{0,16},{16,0},{1,17},{17,1},{2,18},{18,2},{3,19},{19,3},{4,20},{20... | collective-permute-start | bytes 1572872 | tf_op jit(solution)/shard_map/ppermute | solution.py:67
  360.6 30.5 %collective-permute-start.49 = (bf16[256,1024]{1,0:T(8,128)(2,1)S(1)}, bf16[256,1024]{1,0:T(8,128)(2,1)S(1)}, u32[]{:S(2)}, u32[]{:S(2)}) collective-permute-start(bf16[256,1024]{1,0:T(8,128)(2,1)S(1)} %collective-permute-done.47), channel_id=1, source_target_pairs={{0,4},{4,8},{8,12},{12,0},{1,5},{5,9},{9,13},{13,1},{2,6},{6,10},{... | collective-permute-start | bytes 1572872 | tf_op jit(solution)/shard_map/ppermute | solution.py:64
  368.6 23.9 %collective-permute-start.42 = (bf16[1024,256]{1,0:T(8,128)(2,1)S(1)}, bf16[1024,256]{1,0:T(8,128)(2,1)S(1)}, u32[]{:S(2)}, u32[]{:S(2)}) collective-permute-start(bf16[1024,256]{1,0:T(8,128)(2,1)S(1)} %collective-permute-done.41), channel_id=1, source_target_pairs={{0,16},{16,0},{1,17},{17,1},{2,18},{18,2},{3,19},{19,3},{4,20},{20... | collective-permute-start | bytes 1572872 | tf_op jit(solution)/shard_map/ppermute | solution.py:67
  371.8 30.5 %collective-permute-start.43 = (bf16[1024,256]{1,0:T(8,128)(2,1)S(1)}, bf16[1024,256]{1,0:T(8,128)(2,1)S(1)}, u32[]{:S(2)}, u32[]{:S(2)}) collective-permute-start(bf16[1024,256]{1,0:T(8,128)(2,1)S(1)} %collective-permute-done.41), channel_id=1, source_target_pairs={{0,4},{4,8},{8,12},{12,0},{1,5},{5,9},{9,13},{13,1},{2,6},{6,10},{... | collective-permute-start | bytes 1572872 | tf_op jit(solution)/shard_map/ppermute | solution.py:64
  379.8 24.8 %collective-permute-start.30 = (bf16[1024,256]{1,0:T(8,128)(2,1)S(1)}, bf16[1024,256]{1,0:T(8,128)(2,1)S(1)}, u32[]{:S(2)}, u32[]{:S(2)}) collective-permute-start(bf16[1024,256]{1,0:T(8,128)(2,1)S(1)} %collective-permute-done.29), channel_id=1, source_target_pairs={{0,16},{16,0},{1,17},{17,1},{2,18},{18,2},{3,19},{19,3},{4,20},{20... | collective-permute-start | bytes 1572872 | tf_op jit(solution)/shard_map/ppermute | solution.py:67
  381.3 32.3 %collective-permute-start.31 = (bf16[1024,256]{1,0:T(8,128)(2,1)S(1)}, bf16[1024,256]{1,0:T(8,128)(2,1)S(1)}, u32[]{:S(2)}, u32[]{:S(2)}) collective-permute-start(bf16[1024,256]{1,0:T(8,128)(2,1)S(1)} %collective-permute-done.29), channel_id=1, source_target_pairs={{0,4},{4,8},{8,12},{12,0},{1,5},{5,9},{9,13},{13,1},{2,6},{6,10},{... | collective-permute-start | bytes 1572872 | tf_op jit(solution)/shard_map/ppermute | solution.py:64
  391.1 33.9 %collective-permute-start.36 = (bf16[256,1024]{1,0:T(8,128)(2,1)S(1)}, bf16[256,1024]{1,0:T(8,128)(2,1)S(1)}, u32[]{:S(2)}, u32[]{:S(2)}) collective-permute-start(bf16[256,1024]{1,0:T(8,128)(2,1)S(1)} %collective-permute-done.35), channel_id=1, source_target_pairs={{0,16},{16,0},{1,17},{17,1},{2,18},{18,2},{3,19},{19,3},{4,20},{20... | collective-permute-start | bytes 1572872 | tf_op jit(solution)/shard_map/ppermute | solution.py:67
  392.5 30.9 %collective-permute-start.37 = (bf16[256,1024]{1,0:T(8,128)(2,1)S(1)}, bf16[256,1024]{1,0:T(8,128)(2,1)S(1)}, u32[]{:S(2)}, u32[]{:S(2)}) collective-permute-start(bf16[256,1024]{1,0:T(8,128)(2,1)S(1)} %collective-permute-done.35), channel_id=1, source_target_pairs={{0,4},{4,8},{8,12},{12,0},{1,5},{5,9},{9,13},{13,1},{2,6},{6,10},{... | collective-permute-start | bytes 1572872 | tf_op jit(solution)/shard_map/ppermute | solution.py:64
  402.3 24.3 %collective-permute-start.50 = (bf16[256,1024]{1,0:T(8,128)(2,1)S(1)}, bf16[256,1024]{1,0:T(8,128)(2,1)S(1)}, u32[]{:S(2)}, u32[]{:S(2)}) collective-permute-start(bf16[256,1024]{1,0:T(8,128)(2,1)S(1)} %collective-permute-done.49), channel_id=1, source_target_pairs={{0,16},{16,0},{1,17},{17,1},{2,18},{18,2},{3,19},{19,3},{4,20},{20... | collective-permute-start | bytes 1572872 | tf_op jit(solution)/shard_map/ppermute | solution.py:67
  404.6 23.7 %collective-permute-start.44 = (bf16[1024,256]{1,0:T(8,128)(2,1)S(1)}, bf16[1024,256]{1,0:T(8,128)(2,1)S(1)}, u32[]{:S(2)}, u32[]{:S(2)}) collective-permute-start(bf16[1024,256]{1,0:T(8,128)(2,1)S(1)} %collective-permute-done.43), channel_id=1, source_target_pairs={{0,16},{16,0},{1,17},{17,1},{2,18},{18,2},{3,19},{19,3},{4,20},{20... | collective-permute-start | bytes 1572872 | tf_op jit(solution)/shard_map/ppermute | solution.py:67
  413.5 26.0 %collective-permute-start.32 = (bf16[1024,256]{1,0:T(8,128)(2,1)S(1)}, bf16[1024,256]{1,0:T(8,128)(2,1)S(1)}, u32[]{:S(2)}, u32[]{:S(2)}) collective-permute-start(bf16[1024,256]{1,0:T(8,128)(2,1)S(1)} %collective-permute-done.31), channel_id=1, source_target_pairs={{0,16},{16,0},{1,17},{17,1},{2,18},{18,2},{3,19},{19,3},{4,20},{20... | collective-permute-start | bytes 1572872 | tf_op jit(solution)/shard_map/ppermute | solution.py:67
  423.4 23.9 %collective-permute-start.38 = (bf16[256,1024]{1,0:T(8,128)(2,1)S(1)}, bf16[256,1024]{1,0:T(8,128)(2,1)S(1)}, u32[]{:S(2)}, u32[]{:S(2)}) collective-permute-start(bf16[256,1024]{1,0:T(8,128)(2,1)S(1)} %collective-permute-done.37), channel_id=1, source_target_pairs={{0,16},{16,0},{1,17},{17,1},{2,18},{18,2},{3,19},{19,3},{4,20},{20... | collective-permute-start | bytes 1572872 | tf_op jit(solution)/shard_map/ppermute | solution.py:67
  425.8 25.1 %copy-start.15 = (f32[2048]{0:T(1024)S(1)}, f32[2048]{0:T(1024)}, u32[]{:S(2)}) copy-start(f32[2048]{0:T(1024)} %param.21) | copy-start | bytes 24580
  426.7 20.6 %copy-start.10 = (bf16[2048,1024]{1,0:T(8,128)(2,1)}, bf16[2048,1024]{1,0:T(8,128)(2,1)S(1)}, u32[]{:S(2)}) copy-start(bf16[2048,1024]{1,0:T(8,128)(2,1)S(1)} %constant_dynamic-update-slice_fusion.30) | copy-start | bytes 12582916
  467.2 51.6 %copy-start.2 = (bf16[512,768]{1,0:T(8,128)(2,1)S(1)}, bf16[512,768]{1,0:T(8,128)(2,1)}, u32[]{:S(2)}) copy-start(bf16[512,768]{1,0:T(8,128)(2,1)} %add_convert_fusion.1) | copy-start | bytes 2359300
  (16 other events, 67.4 us)
Sparse Core Ops, SparseCore 0:
  13.6 28.7 all-gather.2
  243.5 35.8 reduce-scatter.2
  281.7 28.4 all-gather.4
  482.6 36.1 reduce-scatter.4
